TPU v7x, 32 devices: a whole 2x2x4 slice. The times are simulated.
32 devices in a mesh: kv: 8 (over z, y), tp: 4 (over x, core).
Axes of the slice: x: 2, y: 2, z: 4, core: 2. Of those that a mesh axis runs over, the one named last changes fastest.
Arguments:
- hidden_in: bfloat16 [16, 4096], P(None, ('kv', 'tp')), may hold values from -12 to 12
- attn_gain: float32 [4096], P('kv'), may hold values from 0.1 to 1.9
- query_weight: bfloat16 [4096, 4096], P('kv', 'tp'), may hold values from -0.09375 to 0.09375
- key_cache: bfloat16 [16, 8192, 8, 128], P(None, 'kv', 'tp'), may hold values from -600 to 600
- value_cache: bfloat16 [16, 8192, 8, 128], P(None, 'kv', 'tp'), may hold values from -6 to 6
- lambdas: float32 [32], P('tp'), may hold values from 0.3 to 0.8
- head_gain: float32 [128], replicated, may hold values from 0.1 to 1.9
- out_weight: bfloat16 [4096, 4096], P('tp', 'kv'), may hold values from -0.09375 to 0.09375
- mixer_gain: float32 [4096], P(('kv', 'tp')), may hold values from 0.1 to 1.9
- gate_weight: bfloat16 [4096, 11264], P('kv', 'tp'), may hold values from -0.09375 to 0.09375
- up_weight: bfloat16 [4096, 11264], P('kv', 'tp'), may hold values from -0.09375 to 0.09375
- down_weight: bfloat16 [11264, 4096], P('tp', 'kv'), may hold values from -0.0546875 to 0.0546875
Outputs:
- mixed: bfloat16 [16, 4096], P(None, ('kv', 'tp'))
All inputs are finite; a program needn't handle non-finite values.
Results may differ from a plain program's by a relative error of at most 0.017.
Values may be sent and summed in bfloat16 or wider, within the bound.
A program may use at most 64 MiB of HBM per device.

v0:
```python
import jax
import jax.numpy as jnp
from jax import lax
from jax.sharding import PartitionSpec as P

D = 4096
HEAD_DIM = 64
eps = 1e-06


def finish_heads(totals, weighted, lambdas, head_gain, kv_dev, group_size):
    head_means = weighted / totals[..., None]
    mixing = lambdas.reshape(kv_dev, group_size)
    attended = head_means[0] - mixing[None, :, :, None] * head_means[1]
    norm_inv = lax.rsqrt(jnp.mean(attended * attended, axis=-1, keepdims=True) + eps)
    head_out = (attended * norm_inv * head_gain).astype(jnp.bfloat16)
    return head_out.reshape(head_out.shape[0], kv_dev * group_size * 2 * HEAD_DIM)


def per_device(
    hidden_in,
    attn_gain,
    query_weight,
    key_cache,
    value_cache,
    lambdas,
    head_gain,
    out_weight,
    mixer_gain,
    gate_weight,
    up_weight,
    down_weight,
):
    batch_rows = hidden_in.shape[0]
    rows_block = lax.all_gather(hidden_in, "tp", axis=1, tiled=True)
    block_f = rows_block.astype(jnp.float32)
    gained = (block_f * attn_gain).astype(jnp.bfloat16)
    partial_value = jnp.dot(gained, query_weight, preferred_element_type=jnp.float32)
    own_cols = hidden_in.astype(jnp.float32)
    squares = lax.psum(jnp.sum(own_cols * own_cols, axis=1), ("kv", "tp"))
    query_full = lax.psum(partial_value, "kv")
    row_scale = lax.rsqrt(squares / D + eps)
    query_rows = (query_full * row_scale[:, None]).astype(jnp.bfloat16)
    positions = key_cache.shape[1]
    kv_dev = key_cache.shape[2]
    heads_dev = query_rows.shape[1] // (2 * HEAD_DIM)
    group_size = heads_dev // kv_dev
    query_heads = query_rows.reshape(batch_rows, kv_dev, group_size, 2, HEAD_DIM)
    key_rows = key_cache.reshape(batch_rows, positions, kv_dev, 2, HEAD_DIM)
    scores = jnp.einsum(
        "bkgcd,bpkcd->cbkgp", query_heads, key_rows, preferred_element_type=jnp.float32
    ) * HEAD_DIM ** (-0.5)
    maxima = jnp.max(scores, axis=-1)
    exponent = jnp.exp(scores - maxima[..., None])
    totals = jnp.sum(exponent, axis=-1)
    exp_weights = exponent.astype(jnp.bfloat16)
    weighted = jnp.einsum(
        "cbkgp,bpkv->cbkgv", exp_weights, value_cache, preferred_element_type=jnp.float32
    )
    parts_max, parts_tot, parts_acc = (
        lax.all_to_all(maxima[None], "kv", split_axis=2, concat_axis=0, tiled=True),
        lax.all_to_all(totals[None], "kv", split_axis=2, concat_axis=0, tiled=True),
        lax.all_to_all(weighted[None], "kv", split_axis=2, concat_axis=0, tiled=True),
    )
    top = jnp.max(parts_max, axis=0)
    factors = jnp.exp(parts_max - top[None])
    own_tot = jnp.sum(parts_tot * factors, axis=0)
    own_acc = jnp.sum(parts_acc * factors[..., None], axis=0)
    own_out = finish_heads(own_tot, own_acc, lambdas, head_gain, kv_dev, group_size)
    head_out = lax.all_gather(own_out, "kv", axis=0, tiled=True)
    projected = jnp.dot(head_out, out_weight, preferred_element_type=jnp.float32)
    attn_out = lax.psum_scatter(
        projected.astype(jnp.bfloat16), "tp", scatter_dimension=1, tiled=True
    ).astype(jnp.float32)
    after_attn = (hidden_in.astype(jnp.float32) + attn_out).astype(jnp.bfloat16)
    after_f = after_attn.astype(jnp.float32)
    squares_two = lax.psum(jnp.sum(after_f * after_f, axis=1), ("kv", "tp"))
    mixer_in = (after_f * lax.rsqrt(squares_two / D + eps)[:, None] * mixer_gain).astype(
        jnp.bfloat16
    )
    gathered = lax.all_gather(mixer_in, "tp", axis=1, tiled=True)
    gate_part = jnp.dot(gathered, gate_weight, preferred_element_type=jnp.float32)
    up_part = jnp.dot(gathered, up_weight, preferred_element_type=jnp.float32)
    gate_sum, up_sum = lax.psum((gate_part, up_part), "kv")
    hidden = (jax.nn.silu(gate_sum) * up_sum).astype(jnp.bfloat16)
    down_part = jnp.dot(hidden, down_weight, preferred_element_type=jnp.float32)
    mixer_out = lax.psum_scatter(
        down_part.astype(jnp.bfloat16), "tp", scatter_dimension=1, tiled=True
    ).astype(jnp.float32)
    return (after_f + mixer_out).astype(jnp.bfloat16)


def solution(mesh):
    in_specs = (
        P(None, ("kv", "tp")),
        P("kv"),
        P("kv", "tp"),
        P(None, "kv", "tp", None),
        P(None, "kv", "tp", None),
        P("tp"),
        P(),
        P("tp", "kv"),
        P(("kv", "tp")),
        P("kv", "tp"),
        P("kv", "tp"),
        P("tp", "kv"),
    )
    out_specs = P(None, ("kv", "tp"))
    return jax.shard_map(
        per_device, mesh=mesh, in_specs=in_specs, out_specs=out_specs, check_vma=False
    )
```

profile of v0, /device:TPU:0, one launch (start us, length us, event | category | flops | bytes accessed | tf_op | source)
XLA Modules:
  0.0 329.5 jit_solution(1171620726180046008)
XLA Ops:
  6.5 6.5 %all_gather.9 = bf16[16,512]{1,0:T(8,128)(2,1)S(1)} all-gather(bf16[16,128]{1,0:T(8,128)(2,1)} %param.12), channel_id=1, replica_groups=mesh['kv'=8,'tp'=4] {'tp'}, dimensions={1}, use_global_device_ids=true | all-gather | bytes 20480 | tf_op jit(solution)/shard_map/all_gather | solution.py:35
  13.8 2.1 fusion.15
  16.0 41.0 %psum.36 = f32[16]{0:T(128)S(1)} all-reduce(f32[16]{0:T(128)S(1)} %fusion.17), channel_id=1, replica_groups=mesh['kv'=8,'tp'=4] {'kv','tp'}, use_global_device_ids=true, to_apply=%region_2.0 | all-reduce | flops 16 | bytes 128 | tf_op jit(solution)/shard_map/psum | solution.py:40
  57.0 21.2 %copy.33 = bf16[16,1024,2,128]{1,3,2,0:T(8,128)(2,1)} copy(bf16[16,1024,2,128]{3,2,1,0:T(2,128)(2,1)} %param.15) | data formatting | bytes 16777216 | tf_op args[3]
  78.2 9.0 %all-reduce.4.cloned.1.call-done = f32[16,1024]{1,0:T(8,128)} async-done(((f32[16,1024]{1,0:T(8,128)}), f32[16,1024]{1,0:T(8,128)}) %all-reduce.4.cloned.1.call-update) | async-done | bytes 65552 | tf_op jit(solution)/shard_map/psum | solution.py:41
  87.1 0.9 multiply_convert_fusion.2
  88.2 4.7 %fusion.28 = (f32[2,16,2,4]{3,2,1,0:T(2,128)S(1)}, f32[2,16,2,4,1024]{4,3,2,1,0:T(4,128)S(1)}) fusion(bf16[16,1024,2,2,64]{1,4,3,2,0:T(8,128)(2,1)} %bitcast.56, bf16[16,2,4,2,64]{4,3,2,1,0:T(2,128)(2,1)S(1)} %reshape.35), kind=kOutput, calls=%fused_computation.46 | convolution fusion | flops 34078464 | bytes 9470976 | tf_op jit(solution)/shard_map/bkgcd,bpkcd->cbkgp/dot_general | solution.py:50
  94.1 4.5 %all-to-all-start.2 = ((f32[1,2,16,2,4]{4,3,1,0,2:T(2,128)}), f32[1,2,16,2,4]{4,3,1,0,2:T(2,128)S(1)}, u32[]{:S(2)}, u32[]{:S(2)}) async-start(f32[1,2,16,2,4]{4,3,1,0,2:T(2,128)} %copy.41), calls=%async_computation.2 | async-start | bytes 65536 | tf_op jit(solution)/shard_map/all_to_all | solution.py:62
  99.3 6.1 %all-to-all-done.2 = f32[1,2,16,2,4]{4,3,1,0,2:T(2,128)S(1)} async-done(((f32[1,2,16,2,4]{4,3,1,0,2:T(2,128)}), f32[1,2,16,2,4]{4,3,1,0,2:T(2,128)S(1)}, u32[]{:S(2)}, u32[]{:S(2)}) %all-to-all-start.2) | async-done | bytes 1056 | tf_op jit(solution)/shard_map/all_to_all | solution.py:62
  105.3 3.3 %all-to-all-start.1 = ((f32[1,2,16,2,4]{4,3,1,0,2:T(2,128)}), f32[1,2,16,2,4]{4,3,1,0,2:T(2,128)S(1)}, u32[]{:S(2)}, u32[]{:S(2)}) async-start(f32[1,2,16,2,4]{4,3,1,0,2:T(2,128)} %copy.39), calls=%async_computation.1 | async-start | bytes 65536 | tf_op jit(solution)/shard_map/all_to_all | solution.py:61
  108.7 5.5 %fusion.7 = f32[1,2,16,2,4,128]{5,4,1,3,0,2:T(4,128)} fusion(bf16[16,1024,2,128,1]{3,2,1,0,4:T(2,128)(2,1)} %bitcast.69, bf16[2,16,2,4,1024]{4,3,2,1,0:T(4,128)(2,1)S(1)} %get-tuple-element.10), kind=kOutput, calls=%fused_computation.5 | convolution fusion | flops 67108864 | bytes 9043968 | tf_op jit(solution)/shard_map/cbkgp,bpkv->cbkgv/dot_general | solution.py:57
  114.2 1.1 all-to-all-done.1
  115.3 4.8 %all-to-all-start = ((f32[1,2,16,2,4,128]{5,4,1,3,0,2:T(4,128)}), f32[1,2,16,2,4,128]{5,4,1,3,0,2:T(4,128)S(1)}, u32[]{:S(2)}, u32[]{:S(2)}) async-start(f32[1,2,16,2,4,128]{5,4,1,3,0,2:T(4,128)} %fusion.7), calls=%async_computation | async-start | bytes 262144 | tf_op jit(solution)/shard_map/all_to_all | solution.py:63
  120.4 7.1 %all-to-all-done = f32[1,2,16,2,4,128]{5,4,1,3,0,2:T(4,128)S(1)} async-done(((f32[1,2,16,2,4,128]{5,4,1,3,0,2:T(4,128)}), f32[1,2,16,2,4,128]{5,4,1,3,0,2:T(4,128)S(1)}, u32[]{:S(2)}, u32[]{:S(2)}) %all-to-all-start) | async-done | bytes 131104 | tf_op jit(solution)/shard_map/all_to_all | solution.py:63
  128.1 30.6 %all-gather = bf16[8,2,1024]{2,1,0:T(2,128)(2,1)S(1)} all-gather(bf16[1,2,1024]{2,1,0:T(2,128)(2,1)S(1)} %fusion.25), channel_id=1, replica_groups=mesh['kv'=8,'tp'=4] {'kv'}, dimensions={0}, use_global_device_ids=true | all-gather | bytes 36864 | tf_op jit(solution)/shard_map/all_gather | solution.py:70
  158.8 1.5 convolution_convert_fusion.1
  161.1 17.5 %reduce-scatter.7.cloned.1.call-done = bf16[128,16]{1,0:T(8,128)(2,1)} async-done(((bf16[512,16]{1,0:T(8,128)(2,1)}), bf16[128,16]{1,0:T(8,128)(2,1)}) %reduce-scatter.7.cloned.1.call-update) | async-done | bytes 4112
  179.5 39.3 %psum.37 = f32[16]{0:T(128)S(1)} all-reduce(f32[16]{0:T(128)S(1)} %fusion.19), channel_id=1, replica_groups=mesh['kv'=8,'tp'=4] {'kv','tp'}, use_global_device_ids=true, to_apply=%region_11.0 | all-reduce | flops 16 | bytes 128 | tf_op jit(solution)/shard_map/psum | solution.py:77
  218.9 5.6 %all_gather.11 = bf16[16,512]{1,0:T(8,128)(2,1)S(1)} all-gather(bf16[16,128]{1,0:T(8,128)(2,1)S(1)} %fusion.21), channel_id=1, replica_groups=mesh['kv'=8,'tp'=4] {'tp'}, dimensions={1}, use_global_device_ids=true | all-gather | bytes 20480 | tf_op jit(solution)/shard_map/all_gather | solution.py:81
  224.5 1.2 fusion.29
  225.6 1.2 fusion.30
  226.9 72.3 %all-reduce.6.cloned.1.call-done = (f32[16,2816]{1,0:T(8,128)}, f32[16,2816]{1,0:T(8,128)}) async-done(((f32[16,2816]{1,0:T(8,128)}, f32[16,2816]{1,0:T(8,128)}), (f32[16,2816]{1,0:T(8,128)}, f32[16,2816]{1,0:T(8,128)})) %all-reduce.6.cloned.1.call-update) | async-done | bytes 360464 | tf_op jit(solution)/shard_map/psum | solution.py:84
  299.2 2.5 convolution_convert_fusion
  302.5 19.1 %reduce-scatter.9.cloned.1.call-done = bf16[128,16]{1,0:T(8,128)(2,1)} async-done(((bf16[512,16]{1,0:T(8,128)(2,1)}), bf16[128,16]{1,0:T(8,128)(2,1)}) %reduce-scatter.9.cloned.1.call-update) | async-done | bytes 4112
  (52 shorter events, 7.8 us)
Async XLA Ops:
  6.5 217.9 %copy-start = (bf16[512,2816]{1,0:T(8,128)(2,1)S(1)}, bf16[512,2816]{1,0:T(8,128)(2,1)}, u32[]{:S(2)}) copy-start(bf16[512,2816]{1,0:T(8,128)(2,1)} %param.21) | copy-start | bytes 8650756
  6.5 80.6 %all-reduce.4.cloned.1.call-start = ((), (), s32[]{:S(2)}) async-start(), calls=%async_computation.5 | async-start | bytes 131072 | tf_op jit(solution)/shard_map/psum | solution.py:41
  94.1 11.2 %all-to-all-start.2 = ((f32[1,2,16,2,4]{4,3,1,0,2:T(2,128)}), f32[1,2,16,2,4]{4,3,1,0,2:T(2,128)S(1)}, u32[]{:S(2)}, u32[]{:S(2)}) async-start(f32[1,2,16,2,4]{4,3,1,0,2:T(2,128)} %copy.41), calls=%async_computation.2 | async-start | bytes 65536 | tf_op jit(solution)/shard_map/all_to_all | solution.py:62
  105.3 10.0 %all-to-all-start.1 = ((f32[1,2,16,2,4]{4,3,1,0,2:T(2,128)}), f32[1,2,16,2,4]{4,3,1,0,2:T(2,128)S(1)}, u32[]{:S(2)}, u32[]{:S(2)}) async-start(f32[1,2,16,2,4]{4,3,1,0,2:T(2,128)} %copy.39), calls=%async_computation.1 | async-start | bytes 65536 | tf_op jit(solution)/shard_map/all_to_all | solution.py:61
  108.7 11.5 %copy-start.5 = (f32[8]{0:T(128)S(1)}, f32[8]{0:T(128)}, u32[]{:S(2)}) copy-start(f32[8]{0:T(128)} %param.17) | copy-start | bytes 100
  108.7 19.4 %copy-start.3 = (f32[128]{0:T(128)S(1)}, f32[128]{0:T(128)}, u32[]{:S(2)}) copy-start(f32[128]{0:T(128)} %param.18) | copy-start | bytes 1540
  108.7 70.7 %copy-start.2 = (bf16[16,128]{1,0:T(8,128)(2,1)S(1)}, bf16[16,128]{1,0:T(8,128)(2,1)}, u32[]{:S(2)}) copy-start(bf16[16,128]{1,0:T(8,128)(2,1)} %param.12) | copy-start | bytes 12292
  108.7 110.1 %copy-start.4 = (f32[128]{0:T(128)S(1)}, f32[128]{0:T(128)}, u32[]{:S(2)}) copy-start(f32[128]{0:T(128)} %param.20) | copy-start | bytes 1540
  115.3 12.2 %all-to-all-start = ((f32[1,2,16,2,4,128]{5,4,1,3,0,2:T(4,128)}), f32[1,2,16,2,4,128]{5,4,1,3,0,2:T(4,128)S(1)}, u32[]{:S(2)}, u32[]{:S(2)}) async-start(f32[1,2,16,2,4,128]{5,4,1,3,0,2:T(4,128)} %fusion.7), calls=%async_computation | async-start | bytes 262144 | tf_op jit(solution)/shard_map/all_to_all | solution.py:63
  120.1 58.4 %reduce-scatter.7.cloned.1.call-start = ((), (), s32[]{:S(2)}) async-start(), calls=%async_computation.6 | async-start | bytes 163840
  161.0 138.2 %all-reduce.6.cloned.1.call-start = ((), (), s32[]{:S(2)}) async-start(), calls=%async_computation.8 | async-start | bytes 720896 | tf_op jit(solution)/shard_map/psum | solution.py:84
  218.8 6.8 %copy-start.1 = (bf16[512,2816]{1,0:T(8,128)(2,1)S(1)}, bf16[512,2816]{1,0:T(8,128)(2,1)}, u32[]{:S(2)}) copy-start(bf16[512,2816]{1,0:T(8,128)(2,1)} %param.22) | copy-start | bytes 8650756
  226.8 94.8 %reduce-scatter.9.cloned.1.call-start = ((), (), s32[]{:S(2)}) async-start(), calls=%async_computation.7 | async-start | bytes 163840
Sparse Core Ops, SparseCore 0:
  16.1 71.0 all-reduce.3
  161.1 17.3 reduce-scatter.6
  226.9 72.2 all-reduce.5
  302.6 18.9 reduce-scatter.8
where the time goes:
time: 331 us; the launch traced here: 330 us
  waiting for transfers between devices  132 us (40%)
  blocking collectives  123 us (37%)
  local copies, waits for them, and re-layouts  26 us (8%)
  matrix products  18.6 us (6%)
  between operations  13.3 us (4%)
  starting transfers between devices  12.8 us (4%)
  other arithmetic  3.66 us (1%)
    psum x1, waiting for transfers between devices, per_device(): gate_sum, up_sum = lax.psum((gate_part, up_part), 'kv')  72.3 us
    psum x1, blocking collectives, per_device(): squares = lax.psum(jnp.sum(own_cols * own_cols, axis=1), ('kv', 'tp'))  41 us
    psum x1, blocking collectives, per_device(): squares_two = lax.psum(jnp.sum(after_f * after_f, axis=1), ('kv', 'tp'))  39.3 us
    unnamed x6, waiting for transfers between devices  36.7 us
    all_gather x1, blocking collectives, per_device(): head_out = lax.all_gather(own_out, 'kv', axis=0, tiled=True)  30.6 us
    unnamed x18, local copies, waits for them, and re-layouts  24.3 us
    psum x1, waiting for transfers between devices, per_device(): query_full = lax.psum(partial_value, 'kv')  8.99 us
    all_to_all x1, waiting for transfers between devices, per_device(): lax.all_to_all(weighted[None], 'kv', split_axis=2, concat_axis=0, tiled=T...  7.09 us
  transfers between devices with their start and end apart: 7, of which 7 were waited for; matrix products, arithmetic and copies ran while one was open for 8% of the time, Pallas kernels for 0%

commit v1 on v0

--- a/solution.py
+++ b/solution.py
@@ -74,7 +74,7 @@
     ).astype(jnp.float32)
     after_attn = (hidden_in.astype(jnp.float32) + attn_out).astype(jnp.bfloat16)
     after_f = after_attn.astype(jnp.float32)
-    squares_two = lax.psum(jnp.sum(after_f * after_f, axis=1), ("kv", "tp"))
+    squares_two = jnp.sum(lax.all_gather(jnp.sum(after_f * after_f, axis=1), ("kv", "tp")), axis=0)
     mixer_in = (after_f * lax.rsqrt(squares_two / D + eps)[:, None] * mixer_gain).astype(
         jnp.bfloat16
     )

time: 331 us -> 331 us (level)
    psum x1 -> x0, blocking collectives: 39.3 us -> none  [per_device(): squares_two = lax.psum(jnp.sum(after_f * after_f, axis=1), ('kv', 'tp'))]
    unnamed x0 -> x1, blocking collectives: none -> 39.2 us
    unnamed x18 -> x20, local copies, waits for them, and re-layouts: 24.3 us -> 24.6 us
where the time goes in v1:
time: 331 us; the launch traced here: 330 us
  waiting for transfers between devices  132 us (40%)
  blocking collectives  123 us (37%)
  local copies, waits for them, and re-layouts  26.3 us (8%)
  matrix products  18.6 us (6%)
  between operations  13.3 us (4%)
  starting transfers between devices  12.8 us (4%)
  other arithmetic  3.69 us (1%)
    psum x1, waiting for transfers between devices, per_device(): gate_sum, up_sum = lax.psum((gate_part, up_part), 'kv')  72.3 us
    psum x1, blocking collectives, per_device(): squares = lax.psum(jnp.sum(own_cols * own_cols, axis=1), ('kv', 'tp'))  41 us
    unnamed x1, blocking collectives  39.2 us
    unnamed x6, waiting for transfers between devices  36.7 us
    all_gather x1, blocking collectives, per_device(): head_out = lax.all_gather(own_out, 'kv', axis=0, tiled=True)  30.6 us
    unnamed x20, local copies, waits for them, and re-layouts  24.6 us
    psum x1, waiting for transfers between devices, per_device(): query_full = lax.psum(partial_value, 'kv')  8.99 us
    all_to_all x1, waiting for transfers between devices, per_device(): lax.all_to_all(weighted[None], 'kv', split_axis=2, concat_axis=0, tiled=T...  7.09 us
  transfers between devices with their start and end apart: 7, of which 7 were waited for; matrix products, arithmetic and copies ran while one was open for 8% of the time, Pallas kernels for 0%

profile of v1, /device:TPU:0, one launch (start us, length us, event | category | flops | bytes accessed | tf_op | source)
XLA Modules:
  0.0 329.9 jit_solution(6588057418720872200)
XLA Ops:
  6.5 6.5 %all_gather.15 = bf16[16,512]{1,0:T(8,128)(2,1)S(1)} all-gather(bf16[16,128]{1,0:T(8,128)(2,1)} %param.12), channel_id=1, replica_groups=mesh['kv'=8,'tp'=4] {'tp'}, dimensions={1}, use_global_device_ids=true | all-gather | bytes 20480 | tf_op jit(solution)/shard_map/all_gather | solution.py:35
  13.8 2.1 fusion.15
  16.0 41.0 %psum.29 = f32[16]{0:T(128)S(1)} all-reduce(f32[16]{0:T(128)S(1)} %fusion.17), channel_id=1, replica_groups=mesh['kv'=8,'tp'=4] {'kv','tp'}, use_global_device_ids=true, to_apply=%region_2.0 | all-reduce | flops 16 | bytes 128 | tf_op jit(solution)/shard_map/psum | solution.py:40
  57.0 21.2 %copy.33 = bf16[16,1024,2,128]{1,3,2,0:T(8,128)(2,1)} copy(bf16[16,1024,2,128]{3,2,1,0:T(2,128)(2,1)} %param.15) | data formatting | bytes 16777216 | tf_op args[3]
  78.2 9.0 %all-reduce.5.cloned.1.call-done = f32[16,1024]{1,0:T(8,128)} async-done(((f32[16,1024]{1,0:T(8,128)}), f32[16,1024]{1,0:T(8,128)}) %all-reduce.5.cloned.1.call-update) | async-done | bytes 65552 | tf_op jit(solution)/shard_map/psum | solution.py:41
  87.1 0.9 multiply_convert_fusion.2
  88.2 4.7 %fusion.28 = (f32[2,16,2,4]{3,2,1,0:T(2,128)S(1)}, f32[2,16,2,4,1024]{4,3,2,1,0:T(4,128)S(1)}) fusion(bf16[16,1024,2,2,64]{1,4,3,2,0:T(8,128)(2,1)} %bitcast.56, bf16[16,2,4,2,64]{4,3,2,1,0:T(2,128)(2,1)S(1)} %reshape.39), kind=kOutput, calls=%fused_computation.46 | convolution fusion | flops 34078464 | bytes 9470976 | tf_op jit(solution)/shard_map/bkgcd,bpkcd->cbkgp/dot_general | solution.py:50
  94.1 4.5 %all-to-all-start.2 = ((f32[1,2,16,2,4]{4,3,1,0,2:T(2,128)}), f32[1,2,16,2,4]{4,3,1,0,2:T(2,128)S(1)}, u32[]{:S(2)}, u32[]{:S(2)}) async-start(f32[1,2,16,2,4]{4,3,1,0,2:T(2,128)} %copy.41), calls=%async_computation.2 | async-start | bytes 65536 | tf_op jit(solution)/shard_map/all_to_all | solution.py:62
  99.3 6.1 %all-to-all-done.2 = f32[1,2,16,2,4]{4,3,1,0,2:T(2,128)S(1)} async-done(((f32[1,2,16,2,4]{4,3,1,0,2:T(2,128)}), f32[1,2,16,2,4]{4,3,1,0,2:T(2,128)S(1)}, u32[]{:S(2)}, u32[]{:S(2)}) %all-to-all-start.2) | async-done | bytes 1056 | tf_op jit(solution)/shard_map/all_to_all | solution.py:62
  105.3 3.3 %all-to-all-start.1 = ((f32[1,2,16,2,4]{4,3,1,0,2:T(2,128)}), f32[1,2,16,2,4]{4,3,1,0,2:T(2,128)S(1)}, u32[]{:S(2)}, u32[]{:S(2)}) async-start(f32[1,2,16,2,4]{4,3,1,0,2:T(2,128)} %copy.39), calls=%async_computation.1 | async-start | bytes 65536 | tf_op jit(solution)/shard_map/all_to_all | solution.py:61
  108.7 5.5 %fusion.7 = f32[1,2,16,2,4,128]{5,4,1,3,0,2:T(4,128)} fusion(bf16[16,1024,2,128,1]{3,2,1,0,4:T(2,128)(2,1)} %bitcast.69, bf16[2,16,2,4,1024]{4,3,2,1,0:T(4,128)(2,1)S(1)} %get-tuple-element.10), kind=kOutput, calls=%fused_computation.5 | convolution fusion | flops 67108864 | bytes 9043968 | tf_op jit(solution)/shard_map/cbkgp,bpkv->cbkgv/dot_general | solution.py:57
  114.2 1.1 all-to-all-done.1
  115.3 4.8 %all-to-all-start = ((f32[1,2,16,2,4,128]{5,4,1,3,0,2:T(4,128)}), f32[1,2,16,2,4,128]{5,4,1,3,0,2:T(4,128)S(1)}, u32[]{:S(2)}, u32[]{:S(2)}) async-start(f32[1,2,16,2,4,128]{5,4,1,3,0,2:T(4,128)} %fusion.7), calls=%async_computation | async-start | bytes 262144 | tf_op jit(solution)/shard_map/all_to_all | solution.py:63
  120.4 7.1 %all-to-all-done = f32[1,2,16,2,4,128]{5,4,1,3,0,2:T(4,128)S(1)} async-done(((f32[1,2,16,2,4,128]{5,4,1,3,0,2:T(4,128)}), f32[1,2,16,2,4,128]{5,4,1,3,0,2:T(4,128)S(1)}, u32[]{:S(2)}, u32[]{:S(2)}) %all-to-all-start) | async-done | bytes 131104 | tf_op jit(solution)/shard_map/all_to_all | solution.py:63
  128.1 30.6 %all-gather.1 = bf16[8,2,1024]{2,1,0:T(2,128)(2,1)S(1)} all-gather(bf16[1,2,1024]{2,1,0:T(2,128)(2,1)S(1)} %fusion.25), channel_id=1, replica_groups=mesh['kv'=8,'tp'=4] {'kv'}, dimensions={0}, use_global_device_ids=true | all-gather | bytes 36864 | tf_op jit(solution)/shard_map/all_gather | solution.py:70
  158.8 1.5 convolution_convert_fusion.1
  161.1 17.5 %reduce-scatter.7.cloned.1.call-done = bf16[128,16]{1,0:T(8,128)(2,1)} async-done(((bf16[512,16]{1,0:T(8,128)(2,1)}), bf16[128,16]{1,0:T(8,128)(2,1)}) %reduce-scatter.7.cloned.1.call-update) | async-done | bytes 4112
  179.8 39.2 %all-reduce = f32[512]{0:T(512)S(1)} all-reduce(f32[512]{0:T(512)S(1)} %dynamic-update-slice), channel_id=2, replica_groups=mesh['kv'=8,'tp'=4] {'kv','tp'}, use_global_device_ids=true, to_apply=%add | all-reduce | flops 512 | bytes 4096
  219.2 5.6 %all_gather.19 = bf16[16,512]{1,0:T(8,128)(2,1)S(1)} all-gather(bf16[16,128]{1,0:T(8,128)(2,1)S(1)} %fusion.21), channel_id=1, replica_groups=mesh['kv'=8,'tp'=4] {'tp'}, dimensions={1}, use_global_device_ids=true | all-gather | bytes 20480 | tf_op jit(solution)/shard_map/all_gather | solution.py:81
  224.8 1.2 fusion.29
  226.0 1.2 fusion.30
  227.2 72.3 %all-reduce.7.cloned.1.call-done = (f32[16,2816]{1,0:T(8,128)}, f32[16,2816]{1,0:T(8,128)}) async-done(((f32[16,2816]{1,0:T(8,128)}, f32[16,2816]{1,0:T(8,128)}), (f32[16,2816]{1,0:T(8,128)}, f32[16,2816]{1,0:T(8,128)})) %all-reduce.7.cloned.1.call-update) | async-done | bytes 360464 | tf_op jit(solution)/shard_map/psum | solution.py:84
  299.5 2.5 convolution_convert_fusion
  302.8 19.1 %reduce-scatter.9.cloned.1.call-done = bf16[128,16]{1,0:T(8,128)(2,1)} async-done(((bf16[512,16]{1,0:T(8,128)(2,1)}), bf16[128,16]{1,0:T(8,128)(2,1)}) %reduce-scatter.9.cloned.1.call-update) | async-done | bytes 4112
  (56 shorter events, 8.1 us)
Async XLA Ops:
  6.5 218.3 %copy-start = (bf16[512,2816]{1,0:T(8,128)(2,1)S(1)}, bf16[512,2816]{1,0:T(8,128)(2,1)}, u32[]{:S(2)}) copy-start(bf16[512,2816]{1,0:T(8,128)(2,1)} %param.21) | copy-start | bytes 8650756
  6.5 80.6 %all-reduce.5.cloned.1.call-start = ((), (), s32[]{:S(2)}) async-start(), calls=%async_computation.5 | async-start | bytes 131072 | tf_op jit(solution)/shard_map/psum | solution.py:41
  94.1 11.2 %all-to-all-start.2 = ((f32[1,2,16,2,4]{4,3,1,0,2:T(2,128)}), f32[1,2,16,2,4]{4,3,1,0,2:T(2,128)S(1)}, u32[]{:S(2)}, u32[]{:S(2)}) async-start(f32[1,2,16,2,4]{4,3,1,0,2:T(2,128)} %copy.41), calls=%async_computation.2 | async-start | bytes 65536 | tf_op jit(solution)/shard_map/all_to_all | solution.py:62
  105.3 10.0 %all-to-all-start.1 = ((f32[1,2,16,2,4]{4,3,1,0,2:T(2,128)}), f32[1,2,16,2,4]{4,3,1,0,2:T(2,128)S(1)}, u32[]{:S(2)}, u32[]{:S(2)}) async-start(f32[1,2,16,2,4]{4,3,1,0,2:T(2,128)} %copy.39), calls=%async_computation.1 | async-start | bytes 65536 | tf_op jit(solution)/shard_map/all_to_all | solution.py:61
  108.7 11.5 %copy-start.5 = (f32[8]{0:T(128)S(1)}, f32[8]{0:T(128)}, u32[]{:S(2)}) copy-start(f32[8]{0:T(128)} %param.17) | copy-start | bytes 100
  108.7 19.4 %copy-start.3 = (f32[128]{0:T(128)S(1)}, f32[128]{0:T(128)}, u32[]{:S(2)}) copy-start(f32[128]{0:T(128)} %param.18) | copy-start | bytes 1540
  108.7 70.7 %copy-start.2 = (bf16[16,128]{1,0:T(8,128)(2,1)S(1)}, bf16[16,128]{1,0:T(8,128)(2,1)}, u32[]{:S(2)}) copy-start(bf16[16,128]{1,0:T(8,128)(2,1)} %param.12) | copy-start | bytes 12292
  108.7 110.4 %copy-start.4 = (f32[128]{0:T(128)S(1)}, f32[128]{0:T(128)}, u32[]{:S(2)}) copy-start(f32[128]{0:T(128)} %param.20) | copy-start | bytes 1540
  115.3 12.2 %all-to-all-start = ((f32[1,2,16,2,4,128]{5,4,1,3,0,2:T(4,128)}), f32[1,2,16,2,4,128]{5,4,1,3,0,2:T(4,128)S(1)}, u32[]{:S(2)}, u32[]{:S(2)}) async-start(f32[1,2,16,2,4,128]{5,4,1,3,0,2:T(4,128)} %fusion.7), calls=%async_computation | async-start | bytes 262144 | tf_op jit(solution)/shard_map/all_to_all | solution.py:63
  120.1 58.4 %reduce-scatter.7.cloned.1.call-start = ((), (), s32[]{:S(2)}) async-start(), calls=%async_computation.6 | async-start | bytes 163840
  161.0 138.5 %all-reduce.7.cloned.1.call-start = ((), (), s32[]{:S(2)}) async-start(), calls=%async_computation.8 | async-start | bytes 720896 | tf_op jit(solution)/shard_map/psum | solution.py:84
  219.1 6.8 %copy-start.1 = (bf16[512,2816]{1,0:T(8,128)(2,1)S(1)}, bf16[512,2816]{1,0:T(8,128)(2,1)}, u32[]{:S(2)}) copy-start(bf16[512,2816]{1,0:T(8,128)(2,1)} %param.22) | copy-start | bytes 8650756
  227.1 94.8 %reduce-scatter.9.cloned.1.call-start = ((), (), s32[]{:S(2)}) async-start(), calls=%async_computation.7 | async-start | bytes 163840
Sparse Core Ops, SparseCore 0:
  16.1 71.0 all-reduce.4
  161.1 17.3 reduce-scatter.6
  227.3 72.2 all-reduce.6
  302.9 18.9 reduce-scatter.8
